TPU v7x, 32 devices: a whole 2x2x4 slice. The times are simulated.
32 devices in a mesh: rep: 2 (over x), fs: 8 (over z, y), tp: 2 (over core).
Axes of the slice: x: 2, y: 2, z: 4, core: 2. Of those that a mesh axis runs over, the one named last changes fastest.
Arguments:
- x_early: bfloat16 [1792, 2048], P(('rep', 'fs')), may hold values from -6 to 6
- x_late: bfloat16 [1792, 2048], P(('rep', 'fs')), may hold values from -6 to 6
- grad_out: bfloat16 [1792, 2048], P(('rep', 'fs')), may hold values from -6 to 6
- w_gate: bfloat16 [2048, 3072], P('fs', 'tp'), may hold values from -0.125 to 0.125
- w_up: bfloat16 [2048, 3072], P('fs', 'tp'), may hold values from -0.125 to 0.125
- w_down: bfloat16 [3072, 2048], P('tp', 'fs'), may hold values from -0.109375 to 0.109375
- gate_sum: float32 [2048, 3072], P('fs', 'tp'), may hold values from -80 to 80
- up_sum: float32 [2048, 3072], P('fs', 'tp'), may hold values from -80 to 80
- down_sum: float32 [3072, 2048], P('tp', 'fs'), may hold values from -80 to 80
Outputs:
- out_late: bfloat16 [1792, 2048], P(('rep', 'fs'))
- grad_in: bfloat16 [1792, 2048], P(('rep', 'fs'))
- new_gate_sum: float32 [2048, 3072], P('fs', 'tp')
- new_up_sum: float32 [2048, 3072], P('fs', 'tp')
- new_down_sum: float32 [3072, 2048], P('tp', 'fs')
All inputs are finite; a program needn't handle non-finite values.
Results may differ from a plain program's by a relative error of at most 0.018.
Values may be sent and summed in bfloat16 or wider, within the bound.
A program may use at most 128 MiB of HBM per device.

v0:
```python
import jax
import jax.numpy as jnp
from jax import lax
from jax.sharding import PartitionSpec as P

epsilon = 1e-06


def contract_rows(left, right):
    return lax.dot_general(
        left, right, (((0,), (0,)), ((), ())), preferred_element_type=jnp.float32
    )


def contract_cols(left, right):
    return lax.dot_general(
        left, right, (((1,), (1,)), ((), ())), preferred_element_type=jnp.float32
    )


def shards(x_early, x_late, grad_out, w_gate, w_up, w_down, gate_sum, up_sum, down_sum):
    gate_full, up_full, down_full = (
        lax.all_gather(w_gate, "fs", axis=0, tiled=True),
        lax.all_gather(w_up, "fs", axis=0, tiled=True),
        lax.all_gather(w_down, "fs", axis=1, tiled=True),
    )
    batch_rows = x_early.shape[0]
    stacked = jnp.concatenate([x_early, x_late], axis=0).astype(jnp.float32)
    row_scale = lax.rsqrt(jnp.mean(stacked * stacked, axis=-1, keepdims=True) + epsilon)
    normed = (stacked * row_scale).astype(jnp.bfloat16)
    gate_pre = jnp.dot(normed, gate_full, preferred_element_type=jnp.float32)
    up_pre = jnp.dot(normed, up_full, preferred_element_type=jnp.float32)
    gate_sig = jax.nn.sigmoid(gate_pre)
    hidden = (gate_pre * gate_sig * up_pre).astype(jnp.bfloat16)
    late_part = jnp.dot(hidden[batch_rows:], down_full, preferred_element_type=jnp.float32).astype(
        jnp.bfloat16
    )
    branch = lax.psum(late_part, "tp").astype(jnp.float32)
    out_late = (stacked[batch_rows:] + 0.5 * branch).astype(jnp.bfloat16)
    early_gate = gate_pre[:batch_rows]
    early_upper = up_pre[:batch_rows]
    early_sig = gate_sig[:batch_rows]
    early_hidden = hidden[:batch_rows]
    early_normed = normed[:batch_rows]
    early_scale = row_scale[:batch_rows]
    grad_hidden = 0.5 * contract_cols(grad_out, down_full)
    grad_gate_in = (
        grad_hidden * early_upper * early_sig * (1.0 + early_gate * (1.0 - early_sig))
    ).astype(jnp.bfloat16)
    grad_up_in = (grad_hidden * early_gate * early_sig).astype(jnp.bfloat16)
    normed_part = contract_cols(grad_gate_in, gate_full) + contract_cols(grad_up_in, up_full)
    grad_normed = lax.psum(normed_part.astype(jnp.bfloat16), "tp").astype(jnp.float32)
    unit_rows = stacked[:batch_rows] * early_scale
    inner = jnp.mean(grad_normed * unit_rows, axis=-1, keepdims=True)
    grad_in = (
        grad_out.astype(jnp.float32) + early_scale * (grad_normed - unit_rows * inner)
    ).astype(jnp.bfloat16)
    normed_cols, out_cols = (
        lax.all_to_all(early_normed, "fs", split_axis=1, concat_axis=0, tiled=True),
        lax.all_to_all(grad_out, "fs", split_axis=1, concat_axis=0, tiled=True),
    )
    gate_delta = contract_rows(normed_cols, lax.all_gather(grad_gate_in, "fs", axis=0, tiled=True))
    up_delta = contract_rows(normed_cols, lax.all_gather(grad_up_in, "fs", axis=0, tiled=True))
    down_half = contract_rows(lax.all_gather(early_hidden, "fs", axis=0, tiled=True), out_cols)
    down_delta = 0.5 * down_half
    gate_delta, up_delta, down_delta = (
        lax.psum(gate_delta.astype(jnp.bfloat16), "rep").astype(jnp.float32),
        lax.psum(up_delta.astype(jnp.bfloat16), "rep").astype(jnp.float32),
        lax.psum(down_delta.astype(jnp.bfloat16), "rep").astype(jnp.float32),
    )
    return (out_late, grad_in, gate_sum + gate_delta, up_sum + up_delta, down_sum + down_delta)


def solution(mesh):
    placed = (
        P(("rep", "fs"), None),
        P(("rep", "fs"), None),
        P(("rep", "fs"), None),
        P("fs", "tp"),
        P("fs", "tp"),
        P("tp", "fs"),
        P("fs", "tp"),
        P("fs", "tp"),
        P("tp", "fs"),
    )
    return jax.shard_map(
        shards,
        mesh=mesh,
        in_specs=placed,
        out_specs=(
            P(("rep", "fs"), None),
            P(("rep", "fs"), None),
            P("fs", "tp"),
            P("fs", "tp"),
            P("tp", "fs"),
        ),
        check_vma=False,
    )
```

profile of v0, /device:TPU:9, one launch (start us, length us, event | category | flops | bytes accessed | tf_op | source)
XLA Modules:
  0.0 606.4 jit_solution(10017036902288530399)
XLA Ops:
  10.0 97.5 %all-gather.9.cloned.1.call-done = bf16[2048,1536]{1,0:T(8,128)(2,1)} async-done(((bf16[256,1536]{1,0:T(8,128)(2,1)}), bf16[2048,1536]{1,0:T(8,128)(2,1)}) %all-gather.9.cloned.1.call-update) | async-done | bytes 6291472 | tf_op jit(solution)/shard_map/all_gather | solution.py:24
  107.5 5.4 fusion.11
  112.9 93.6 %all-gather.7.cloned.1.call-done = bf16[2048,1536]{1,0:T(8,128)(2,1)} async-done(((bf16[256,1536]{1,0:T(8,128)(2,1)}), bf16[2048,1536]{1,0:T(8,128)(2,1)}) %all-gather.7.cloned.1.call-update) | async-done | bytes 6291472 | tf_op jit(solution)/shard_map/all_gather | solution.py:23
  206.5 6.5 %add_divide_fusion = (f32[224,1536]{1,0:T(8,128)}, bf16[224,1536]{1,0:T(8,128)(2,1)}, f32[224,1536]{1,0:T(8,128)}) fusion(f32[224,1536]{1,0:T(8,128)} %fusion.11, bf16[224,2048]{1,0:T(8,128)(2,1)S(1)} %multiply_convert_fusion, bf16[2048,1536]{1,0:T(8,128)(2,1)} %all-gather.7.cloned.1.call-done), kind=kOutput, calls=%fused_computation.14 | convolution fusion | flops 1411350528 | bytes 12025856 | tf_op jit(solution)/shard_map/dot_general | solution.py:31
  213.1 93.2 %all-gather.11.cloned.1.call-done = bf16[1536,2048]{1,0:T(8,128)(2,1)} async-done(((bf16[1536,256]{1,0:T(8,128)(2,1)}), bf16[1536,2048]{1,0:T(8,128)(2,1)}) %all-gather.11.cloned.1.call-update) | async-done | bytes 6291472 | tf_op jit(solution)/shard_map/all_gather | solution.py:25
  306.3 6.4 %multiply_convert_fusion.2 = (bf16[112,1536]{1,0:T(8,128)(2,1)}, bf16[112,1536]{1,0:T(8,128)(2,1)}) fusion(f32[224,1536]{1,0:T(8,128)} %get-tuple-element.16, f32[224,1536]{1,0:T(8,128)} %get-tuple-element.14, f32[224,1536]{1,0:T(8,128)} %fusion.11, bf16[112,2048]{1,0:T(8,128)(2,1)S(1)} %copy-done, bf16[1536,2048]{1,0:T(8,128)(2,1)} %all-gather.11.cloned.1.call-done), kind=kOutput, calls=%fused_computation.29 | convolution fusion | flops 706535424 | bytes 9502720 | tf_op jit(solution)/shard_map/dot_general | solution.py:16
  313.4 1.9 slice.44
  317.2 6.1 %all-to-all-start = ((bf16[112,8,256]{2,0,1:T(8,128)(2,1)}), bf16[112,8,256]{2,0,1:T(8,128)(2,1)}, u32[]{:S(2)}, u32[]{:S(2)}) async-start(bf16[112,8,256]{2,0,1:T(8,128)(2,1)} %bitcast.35), calls=%async_computation | async-start | bytes 917504 | tf_op jit(solution)/shard_map/all_to_all | solution.py:59
  324.1 5.1 fusion.12
  329.2 2.8 fusion.1
  332.0 11.5 %all-to-all-done = bf16[112,8,256]{2,0,1:T(8,128)(2,1)} async-done(((bf16[112,8,256]{2,0,1:T(8,128)(2,1)}), bf16[112,8,256]{2,0,1:T(8,128)(2,1)}, u32[]{:S(2)}, u32[]{:S(2)}) %all-to-all-start) | async-done | bytes 458784 | tf_op jit(solution)/shard_map/all_to_all | solution.py:59
  343.5 6.5 %all-to-all-start.1 = ((bf16[112,8,256]{2,0,1:T(8,128)(2,1)}), bf16[112,8,256]{2,0,1:T(8,128)(2,1)S(1)}, u32[]{:S(2)}, u32[]{:S(2)}) async-start(bf16[112,8,256]{2,0,1:T(8,128)(2,1)} %bitcast.34), calls=%async_computation.1 | async-start | bytes 917504 | tf_op jit(solution)/shard_map/all_to_all | solution.py:60
  350.0 5.0 convolution_convert_fusion.2
  355.3 27.2 %all-gather.13.cloned.1.call-done = bf16[896,1536]{1,0:T(8,128)(2,1)} async-done(((bf16[112,1536]{1,0:T(8,128)(2,1)}), bf16[896,1536]{1,0:T(8,128)(2,1)}) %all-gather.13.cloned.1.call-update) | async-done | bytes 2752528 | tf_op jit(solution)/shard_map/all_gather | solution.py:62
  382.6 3.8 convolution_convert_fusion.1
  386.4 55.3 %all-gather.15.cloned.1.call-done = bf16[896,1536]{1,0:T(8,128)(2,1)} async-done(((bf16[112,1536]{1,0:T(8,128)(2,1)}), bf16[896,1536]{1,0:T(8,128)(2,1)}) %all-gather.15.cloned.1.call-update) | async-done | bytes 2752528 | tf_op jit(solution)/shard_map/all_gather | solution.py:63
  441.7 3.8 convolution_convert_fusion
  445.5 52.9 %all-gather.17.cloned.1.call-done = bf16[896,1536]{1,0:T(8,128)(2,1)} async-done(((bf16[112,1536]{1,0:T(8,128)(2,1)}), bf16[896,1536]{1,0:T(8,128)(2,1)}) %all-gather.17.cloned.1.call-update) | async-done | bytes 2752528 | tf_op jit(solution)/shard_map/all_gather | solution.py:64
  498.4 3.7 fusion
  502.3 18.8 %all-reduce.5.cloned.1.call-done = (bf16[112,2048]{1,0:T(8,128)(2,1)}, bf16[112,2048]{1,0:T(8,128)(2,1)}) async-done(((bf16[112,2048]{1,0:T(8,128)(2,1)}, bf16[112,2048]{1,0:T(8,128)(2,1)}), (bf16[112,2048]{1,0:T(8,128)(2,1)}, bf16[112,2048]{1,0:T(8,128)(2,1)})) %all-reduce.5.cloned.1.call-update) | async-done | bytes 917520 | tf_op jit(solution)/shard_map/psum | solution.py:38
  522.4 2.5 fusion.5
  525.0 68.2 %all-reduce.7.cloned.1.call-done = (bf16[256,1536]{1,0:T(8,128)(2,1)}, bf16[256,1536]{1,0:T(8,128)(2,1)}, bf16[1536,256]{1,0:T(8,128)(2,1)}) async-done(((bf16[256,1536]{1,0:T(8,128)(2,1)}, bf16[256,1536]{1,0:T(8,128)(2,1)}, bf16[1536,256]{1,0:T(8,128)(2,1)}), (bf16[256,1536]{1,0:T(8,128)(2,1)}, bf16[256,1536]{1,0:T(8,128)(2,1)}, bf16[1536,256]{1,0:T(8,128)(2,1)})) %all-reduce.7.cloned.1.call-update) | async-done | bytes 2359312 | tf_op jit(solution)/shard_map/psum | solution.py:67
  593.2 3.1 convert_add_fusion
  596.3 3.3 convert_add_fusion.1
  (48 shorter events, 7.8 us)
Async XLA Ops:
  7.2 2.3 copy-start.1
  7.2 2.3 copy-start.2
  7.2 100.3 %all-gather.9.cloned.1.call-start = ((), (), s32[]{:S(2)}) async-start(), calls=%async_computation.3 | async-start | bytes 7077888 | tf_op jit(solution)/shard_map/all_gather | solution.py:24
  7.9 198.6 %all-gather.7.cloned.1.call-start = ((), (), s32[]{:S(2)}) async-start(), calls=%async_computation.2 | async-start | bytes 7077888 | tf_op jit(solution)/shard_map/all_gather | solution.py:23
  8.7 297.7 %all-gather.11.cloned.1.call-start = ((), (), s32[]{:S(2)}) async-start(), calls=%async_computation.4 | async-start | bytes 7077888 | tf_op jit(solution)/shard_map/all_gather | solution.py:25
  9.4 373.2 %all-gather.13.cloned.1.call-start = ((), (), s32[]{:S(2)}) async-start(), calls=%async_computation.5 | async-start | bytes 3096576 | tf_op jit(solution)/shard_map/all_gather | solution.py:62
  10.0 196.6 %copy-start.4 = (bf16[224,2048]{1,0:T(8,128)(2,1)}, bf16[224,2048]{1,0:T(8,128)(2,1)S(1)}, u32[]{:S(2)}) copy-start(bf16[224,2048]{1,0:T(8,128)(2,1)S(1)} %multiply_convert_fusion) | copy-start | bytes 2752516
  112.9 193.4 %copy-start = (bf16[112,2048]{1,0:T(8,128)(2,1)S(1)}, bf16[112,2048]{1,0:T(8,128)(2,1)}, u32[]{:S(2)}) copy-start(bf16[112,2048]{1,0:T(8,128)(2,1)} %param.11) | copy-start | bytes 1376260
  312.8 128.9 %all-gather.15.cloned.1.call-start = ((), (), s32[]{:S(2)}) async-start(), calls=%async_computation.6 | async-start | bytes 3096576 | tf_op jit(solution)/shard_map/all_gather | solution.py:63
  313.4 185.0 %all-gather.17.cloned.1.call-start = ((), (), s32[]{:S(2)}) async-start(), calls=%async_computation.7 | async-start | bytes 3096576 | tf_op jit(solution)/shard_map/all_gather | solution.py:64
  313.4 15.8 %slice-start = ((s8[6291456]{0:T(1024)(128)(4,1)}), s8[2097152]{0:T(1024)(128)(4,1)S(1)}, s32[]{:S(2)}) async-start(s8[6291456]{0:T(1024)(128)(4,1)} %bitcast.31), calls=%async_computation.10 | async-start | bytes 4194304
  317.2 26.3 %all-to-all-start = ((bf16[112,8,256]{2,0,1:T(8,128)(2,1)}), bf16[112,8,256]{2,0,1:T(8,128)(2,1)}, u32[]{:S(2)}, u32[]{:S(2)}) async-start(bf16[112,8,256]{2,0,1:T(8,128)(2,1)} %bitcast.35), calls=%async_computation | async-start | bytes 917504 | tf_op jit(solution)/shard_map/all_to_all | solution.py:59
  324.1 5.1 slice-start.1
  324.1 5.1 copy-start.3
  343.5 102.0 %all-to-all-start.1 = ((bf16[112,8,256]{2,0,1:T(8,128)(2,1)}), bf16[112,8,256]{2,0,1:T(8,128)(2,1)S(1)}, u32[]{:S(2)}, u32[]{:S(2)}) async-start(bf16[112,8,256]{2,0,1:T(8,128)(2,1)} %bitcast.34), calls=%async_computation.1 | async-start | bytes 917504 | tf_op jit(solution)/shard_map/all_to_all | solution.py:60
  350.0 171.1 %all-reduce.5.cloned.1.call-start = ((), (), s32[]{:S(2)}) async-start(), calls=%async_computation.8 | async-start | bytes 1835008 | tf_op jit(solution)/shard_map/psum | solution.py:38
  355.1 238.1 %all-reduce.7.cloned.1.call-start = ((), (), s32[]{:S(2)}) async-start(), calls=%async_computation.9 | async-start | bytes 4718592 | tf_op jit(solution)/shard_map/psum | solution.py:67
  593.2 3.1 copy-start.5
  593.2 3.1 copy-start.6
  593.2 3.1 copy-start.7
Sparse Core Ops, SparseCore 0:
  10.2 97.2 all-gather.8
  109.6 96.8 all-gather.6
  208.6 97.6 all-gather.10
  312.9 69.6 all-gather.12
  384.6 57.0 all-gather.14
  443.7 54.5 all-gather.16
  501.3 19.7 all-reduce.4
  524.1 69.0 all-reduce.6
where the time goes:
time: 609 us; the launch traced here: 606 us
  waiting for transfers between devices  521 us (86%)
  matrix products  42.7 us (7%)
  between operations  14.3 us (2%)
  starting transfers between devices  13.1 us (2%)
  other arithmetic  10.9 us (2%)
    all_gather x1, waiting for transfers between devices, shards(): lax.all_gather(w_up, 'fs', axis=0, tiled=True)  97.5 us
    all_gather x1, waiting for transfers between devices, shards(): lax.all_gather(w_gate, 'fs', axis=0, tiled=True)  93.6 us
    all_gather x1, waiting for transfers between devices, shards(): lax.all_gather(w_down, 'fs', axis=1, tiled=True)  93.2 us
    psum x1, waiting for transfers between devices, shards(): lax.psum(gate_delta.astype(jnp.bfloat16), 'rep').astype(jnp.float32)  68.2 us
    all_gather x1, waiting for transfers between devices, shards(): lax.all_gather(grad_up_in, 'fs', axis=0, tiled=True)  55.3 us
    all_gather x1, waiting for transfers between devices, shards(): lax.all_gather(early_hidden, 'fs', axis=0, tiled=True)  52.9 us
    all_gather x1, waiting for transfers between devices, shards(): lax.all_gather(grad_gate_in, 'fs', axis=0, tiled=True)  27.2 us
    psum x1, waiting for transfers between devices, shards(): branch = lax.psum(late_part, 'tp').astype(jnp.float32)  18.8 us
  transfers between devices with their start and end apart: 10, of which 9 were waited for; matrix products, arithmetic and copies ran while one was open for 7% of the time, Pallas kernels for 0%

commit v1 on v0

--- a/solution.py
+++ b/solution.py
@@ -1,9 +1,16 @@
+import functools
+
 import jax
 import jax.numpy as jnp
 from jax import lax
+from jax.experimental import pallas as pl
+from jax.experimental.pallas import tpu as pltpu
 from jax.sharding import PartitionSpec as P
 
 epsilon = 1e-06
+MESH = pl.DeviceIdType.MESH
+ANY = pl.BlockSpec(memory_space=pl.ANY)
+LANES, ROWS = 128, 16
 
 
 def contract_rows(left, right):
@@ -15,6 +22,378 @@
 def contract_cols(left, right):
     return lax.dot_general(
         left, right, (((1,), (1,)), ((), ())), preferred_element_type=jnp.float32
+    )
+
+
+def greet(peers):
+    barrier = pltpu.get_barrier_semaphore()
+    for peer in peers:
+        pl.semaphore_signal(barrier, inc=1, device_id=peer, device_id_type=MESH)
+    pl.semaphore_wait(barrier, len(peers))
+
+
+def push(src, dst, send_sem, recv_sem, peer):
+    copy = pltpu.make_async_remote_copy(
+        src_ref=src,
+        dst_ref=dst,
+        send_sem=send_sem,
+        recv_sem=recv_sem,
+        device_id=peer,
+        device_id_type=MESH,
+    )
+    return copy
+
+
+def block(index, size, unit):
+    return pl.ds(pl.multiple_of(index * size, unit), size)
+
+
+def call(body, outs, sems, collective, *args, scratch=()):
+    return pl.pallas_call(
+        body,
+        out_shape=outs,
+        in_specs=[ANY] * len(args),
+        out_specs=jax.tree.map(lambda _: ANY, outs),
+        scratch_shapes=[pltpu.SemaphoreType.DMA((n,)) for n in sems] + list(scratch),
+        compiler_params=pltpu.CompilerParams(collective_id=collective, has_side_effects=True),
+    )(*args)
+
+
+def here():
+    rep, fs, tp = lax.axis_index("rep"), lax.axis_index("fs"), lax.axis_index("tp")
+    return rep, fs, tp, {"rep": 1 - rep}, {"tp": 1 - tp}
+
+
+def gather_kernel(n, acts, weights, acts_all, weights_all, send, recv, wsend, wrecv):
+    rep, fs, tp, twin, mate = here()
+    line = n // 2
+    z, y = fs // 2, lax.rem(fs, 2)
+    side = {"fs": fs + 1 - 2 * y}
+    rows, width = acts.shape[1], acts.shape[2]
+    half = width // 2
+    piece = weights_all.shape[1]
+    part = piece // 2
+    depth = weights.shape[2]
+    mine = block(tp, half, LANES)
+    greet([twin, mate] + [{"fs": lax.rem(fs + k, n)} for k in range(1, n)])
+
+    def spot(origin):
+        return acts_all.at[:, block(origin, rows, ROWS), mine]
+
+    def other_spot(origin):
+        return acts_all.at[:, block(origin, rows, ROWS), block(1 - tp, half, LANES)]
+
+    right0, left0, side0, mate0 = 1, 1 + line, 1 + 2 * line, 1 + 3 * line
+    own = acts.at[:, :, mine]
+    up, down = {"fs": lax.rem(fs + 2, n)}, {"fs": lax.rem(fs + n - 2, n)}
+
+    def go_up(s):
+        src = own if s == 0 else spot(fs - 2 * s)
+        return push(src, spot(fs - 2 * s), send.at[right0 + s], recv.at[right0 + s], up)
+
+    def go_down(s):
+        src = own if s == 0 else spot(fs + 2 * s)
+        return push(src, spot(fs + 2 * s), send.at[left0 + s], recv.at[left0 + s], down)
+
+    def go_side(s, sign):
+        origin = fs + 2 * sign * s
+        src = own if s == 0 else spot(origin)
+        at = side0 + origin // 2
+        return push(src, spot(origin), send.at[at], recv.at[at], side)
+
+    def go_mate(origin):
+        at = mate0 + origin
+        return push(spot(origin), spot(origin), send.at[at], recv.at[at], mate)
+
+    def weight(k):
+        to = lax.rem(fs + k, n)
+        src = weights.at[:, block(to * 2 + rep, part, ROWS), :]
+        dst = weights_all.at[:, block(rep, part, ROWS), block(fs, depth, LANES)]
+        return push(src, dst, wsend.at[k], wrecv.at[k], {"fs": to})
+
+    def weight_on(k):
+        origin = lax.rem(fs + n - k, n)
+        ref = weights_all.at[:, block(rep, part, ROWS), block(origin, depth, LANES)]
+        return push(ref, ref, wsend.at[n + k], wrecv.at[n + k], twin)
+
+    def weight_from_twin(k):
+        origin = lax.rem(fs + n - k, n)
+        ref = weights_all.at[:, block(1 - rep, part, ROWS), block(origin, depth, LANES)]
+        return push(ref, ref, wsend.at[n + k], wrecv.at[n + k], twin)
+
+    own_weight = push(
+        weights.at[:, block(fs, piece, ROWS), :],
+        weights_all.at[:, :, block(fs, depth, LANES)],
+        wsend.at[0],
+        wrecv.at[0],
+        twin,
+    )
+    own_mate = push(acts, acts_all.at[:, block(fs, rows, ROWS), :], send.at[0], recv.at[0], mate)
+
+    has_up = lambda s: (z - s >= 0) & (z + 1 < line)
+    has_down = lambda s: (z + s < line) & (z - 1 >= 0)
+    from_below = lambda s: z - 1 - s >= 0
+    from_above = lambda s: z + 1 + s < line
+
+    pl.when(has_up(0))(lambda: go_up(0).start())
+    pl.when(has_down(0))(lambda: go_down(0).start())
+    go_side(0, 1).start()
+    own_mate.start()
+    own_weight.start()
+    order = sorted(range(1, n), key=lambda k: -min(k, n - k))
+    groups = [order[g :: line] for g in range(line)]
+
+    for s in range(line - 1):
+        for k in groups[s]:
+            weight(k).start()
+
+        def below():
+            push(spot(fs - 2 * (s + 1)), spot(fs - 2 * (s + 1)), send.at[right0 + s], recv.at[right0 + s], up).wait_recv()
+            if s + 1 < line - 1:
+                pl.when(has_up(s + 1))(lambda: go_up(s + 1).start())
+            go_side(s + 1, -1).start()
+            go_mate(fs - 2 * (s + 1)).start()
+
+        def above():
+            push(spot(fs + 2 * (s + 1)), spot(fs + 2 * (s + 1)), send.at[left0 + s], recv.at[left0 + s], up).wait_recv()
+            if s + 1 < line - 1:
+                pl.when(has_down(s + 1))(lambda: go_down(s + 1).start())
+            go_side(s + 1, 1).start()
+            go_mate(fs + 2 * (s + 1)).start()
+
+        pl.when(from_below(s))(below)
+        pl.when(from_above(s))(above)
+    for k in groups[line - 1]:
+        weight(k).start()
+
+    def side_in(place):
+        origin = place * 2 + (1 - y)
+        at = side0 + place
+        push(spot(origin), spot(origin), send.at[at], recv.at[at], side).wait_recv()
+        go_mate(origin).start()
+
+    side_in(z)
+    for k in order:
+        origin = lax.rem(fs + n - k, n)
+        ref = weights_all.at[:, block(rep, part, ROWS), block(origin, depth, LANES)]
+        push(ref, ref, wsend.at[k], wrecv.at[k], twin).wait_recv()
+        weight_on(k).start()
+    for s in range(1, line):
+        pl.when(z - s >= 0)(lambda: side_in(z - s))
+        pl.when(z + s < line)(lambda: side_in(z + s))
+
+    own_mate.wait()
+    own_weight.wait()
+    for k in range(1, n):
+        weight_from_twin(k).wait_recv()
+        weight_on(k).wait_send()
+        weight(k).wait_send()
+        origin = lax.rem(fs + k, n)
+        at = mate0 + origin
+        ref = other_spot(origin)
+        push(ref, ref, send.at[at], recv.at[at], mate).wait()
+    for s in range(line - 1):
+        pl.when(has_up(s))(lambda: go_up(s).wait_send())
+        pl.when(has_down(s))(lambda: go_down(s).wait_send())
+    for place in range(line):
+        ref = spot(place * 2 + y)
+        push(ref, ref, send.at[side0 + place], recv.at[side0 + place], side).wait_send()
+
+
+def halves_kernel(parts, grads, parts_in, grads_in, send, recv):
+    rep, fs, tp, twin, mate = here()
+    half = parts.shape[2] // 2
+    part = grads.shape[1] // 2
+    greet([twin, mate])
+    one = push(
+        parts.at[:, :, block(1 - tp, half, LANES)], parts_in, send.at[0], recv.at[0], mate
+    )
+    two = push(grads.at[:, block(1 - rep, part, ROWS), :], grads_in, send.at[1], recv.at[1], twin)
+    one.start()
+    two.start()
+    one.wait()
+    two.wait()
+
+
+def pair_kernel(n, parts, grads, parts_in, grads_all, send, recv, stage, local):
+    rep, fs, tp, twin, mate = here()
+    y = lax.rem(fs, 2)
+    side = {"fs": fs + 1 - 2 * y}
+    part = grads.shape[1]
+    depth = grads_all.shape[2]
+    greet([twin] + [{"fs": lax.rem(fs + k, n)} for k in range(1, n)])
+    across = push(parts.at[:, :, 1 - y], parts_in, send.at[0], recv.at[0], side)
+
+    def slot(origin, who):
+        return grads_all.at[:, block(origin * 2 + who, part, ROWS), :]
+
+    def share(k):
+        to = lax.rem(fs + k, n)
+        src = grads.at[:, :, block(to, depth, LANES)]
+        return push(src, slot(fs, rep), send.at[k], recv.at[k], {"fs": to})
+
+    def share_on(k):
+        origin = lax.rem(fs + n - k, n)
+        return push(slot(origin, rep), slot(origin, rep), send.at[n + k], recv.at[n + k], twin)
+
+    def share_from_twin(k):
+        origin = lax.rem(fs + n - k, n)
+        ref = slot(origin, 1 - rep)
+        return push(ref, ref, send.at[n + k], recv.at[n + k], twin)
+
+    order = sorted(range(1, n), key=lambda k: -min(k, n - k))
+    for k in order:
+        share(k).start()
+    across.start()
+    own = grads.at[:, :, block(fs, depth, LANES)]
+    own_twin = push(own, slot(fs, rep), send.at[n], recv.at[n], twin)
+    own_twin.start()
+    take = pltpu.make_async_copy(own, stage, local.at[0])
+    take.start()
+    take.wait()
+    put = pltpu.make_async_copy(stage, slot(fs, rep), local.at[1])
+    put.start()
+    for k in order:
+        origin = lax.rem(fs + n - k, n)
+        ref = slot(origin, rep)
+        push(ref, ref, send.at[k], recv.at[k], twin).wait_recv()
+        share_on(k).start()
+    put.wait()
+    across.wait()
+    own_twin.wait_send()
+    ref = slot(fs, 1 - rep)
+    push(ref, ref, send.at[n], recv.at[n], twin).wait_recv()
+    for k in order:
+        share(k).wait_send()
+        share_on(k).wait_send()
+        share_from_twin(k).wait_recv()
+
+
+def line_kernel(n, parts, parts_in, send, recv):
+    rep, fs, tp, twin, mate = here()
+    line = n // 2
+    z = fs // 2
+    greet([{"fs": lax.rem(fs + 2 * k, n)} for k in range(1, line)])
+
+    def copy(k):
+        to = lax.rem(z + k, line)
+        return push(
+            parts.at[:, to],
+            parts_in.at[k - 1],
+            send.at[k],
+            recv.at[k],
+            {"fs": lax.rem(fs + 2 * k, n)},
+        )
+
+    for k in range(1, line):
+        copy(k).start()
+    for k in range(1, line):
+        copy(k).wait()
+
+
+def mate_kernel(sums, sums_in, send, recv):
+    rep, fs, tp, twin, mate = here()
+    greet([mate])
+    copy = push(sums, sums_in, send.at[0], recv.at[0], mate)
+    copy.start()
+    copy.wait()
+
+
+def fast_shards(n, x_early, x_late, grad_out, w_gate, w_up, w_down, gate_sum, up_sum, down_sum):
+    bf16, f32 = jnp.bfloat16, jnp.float32
+    shape = jax.ShapeDtypeStruct
+    rep, fs, tp = lax.axis_index("rep"), lax.axis_index("fs"), lax.axis_index("tp")
+    line = n // 2
+    y = lax.rem(fs, 2)
+    rows, width = x_early.shape
+    hidden_here, depth = w_down.shape
+    piece = hidden_here // n
+    half = width // 2
+    early = x_early.astype(f32)
+    late = x_late.astype(f32)
+    scale_of = lambda v: lax.rsqrt(jnp.mean(v * v, axis=-1, keepdims=True) + epsilon)
+    early_scale, late_scale = scale_of(early), scale_of(late)
+    acts = jnp.stack(
+        [(early * early_scale).astype(bf16), (late * late_scale).astype(bf16), grad_out]
+    )
+    weights = jnp.stack([w_gate.T, w_up.T, w_down])
+    acts_all, weights_all = call(
+        functools.partial(gather_kernel, n),
+        [shape((3, n * rows, width), bf16), shape((3, piece, width), bf16)],
+        (1 + 3 * line + n, 1 + 3 * line + n, 2 * n, 2 * n),
+        0,
+        acts,
+        weights,
+    )
+    gate_t, up_t, down_t = weights_all[0], weights_all[1], weights_all[2]
+    normed, cotangent = acts_all[0], acts_all[2]
+    gate_up = weights_all[:2].reshape(2 * piece, width)
+    pre = contract_cols(acts_all[:2].reshape(2 * n * rows, width), gate_up)
+    gate_pre, up_pre = pre[:, :piece], pre[:, piece:]
+    sig = jax.nn.sigmoid(gate_pre)
+    hidden = (gate_pre * sig * up_pre).astype(bf16)
+    tokens = n * rows
+    late_part = jnp.dot(hidden[tokens:], down_t, preferred_element_type=f32).astype(bf16)
+    g, u, s = gate_pre[:tokens], up_pre[:tokens], sig[:tokens]
+    grad_hidden = 0.5 * contract_cols(cotangent, down_t)
+    grad_gate_in = (grad_hidden * u * s * (1.0 + g * (1.0 - s))).astype(bf16)
+    grad_up_in = (grad_hidden * g * s).astype(bf16)
+    grads_in = jnp.concatenate([grad_gate_in, grad_up_in], axis=1)
+    normed_part = jnp.dot(grads_in, gate_up, preferred_element_type=f32).astype(bf16)
+    gate_up_delta = contract_rows(grads_in, normed).astype(bf16)
+    down_delta = (0.5 * contract_rows(hidden[:tokens], cotangent)).astype(bf16)
+    grads = jnp.concatenate([gate_up_delta, down_delta], axis=0).reshape(3, piece, width)
+    parts = jnp.stack([late_part, normed_part])
+    parts_in, grads_in = call(
+        halves_kernel,
+        [shape((2, tokens, half), bf16), shape((3, piece // 2, width), bf16)],
+        (2, 2),
+        1,
+        parts,
+        grads,
+    )
+    add = lambda a, b: (a.astype(f32) + b.astype(f32)).astype(bf16)
+    parts = add(lax.dynamic_slice_in_dim(parts, tp * half, half, 2), parts_in)
+    grads = add(lax.dynamic_slice_in_dim(grads, rep * (piece // 2), piece // 2, 1), grads_in)
+    parts = parts.reshape(2, line, 2, rows, half)
+    parts_in, grads_all = call(
+        functools.partial(pair_kernel, n),
+        [shape((2, line, rows, half), bf16), shape((3, hidden_here, depth), bf16)],
+        (2 * n, 2 * n),
+        2,
+        parts,
+        grads,
+        scratch=(
+            pltpu.VMEM((3, piece // 2, depth), bf16),
+            pltpu.SemaphoreType.DMA((2,)),
+        ),
+    )
+    parts = add(lax.dynamic_index_in_dim(parts, y, 2, keepdims=False), parts_in)
+    parts_in = call(
+        functools.partial(line_kernel, n),
+        shape((line - 1, 2, rows, half), bf16),
+        (line, line),
+        3,
+        parts,
+    )
+    sums = lax.dynamic_index_in_dim(parts, fs // 2, 1, keepdims=False).astype(f32)
+    sums = (sums + jnp.sum(parts_in.astype(f32), axis=0)).astype(bf16)
+    sums_in = call(mate_kernel, shape((2, rows, half), bf16), (1, 1), 4, sums)
+    left, right = jnp.where(tp == 0, sums, sums_in), jnp.where(tp == 0, sums_in, sums)
+    full = jnp.concatenate([left, right], axis=2).astype(f32)
+    branch, grad_normed = full[0], full[1]
+    out_late = (late + 0.5 * branch).astype(bf16)
+    unit_rows = early * early_scale
+    inner = jnp.mean(grad_normed * unit_rows, axis=-1, keepdims=True)
+    grad_in = (
+        grad_out.astype(f32) + early_scale * (grad_normed - unit_rows * inner)
+    ).astype(bf16)
+    return (
+        out_late,
+        grad_in,
+        gate_sum + grads_all[0].T.astype(f32),
+        up_sum + grads_all[1].T.astype(f32),
+        down_sum + grads_all[2].astype(f32),
     )
 
 
@@ -71,6 +450,26 @@
     return (out_late, grad_in, gate_sum + gate_delta, up_sum + up_delta, down_sum + down_delta)
 
 
+def shards_for(mesh):
+    n, reps, cores = mesh.shape["fs"], mesh.shape["rep"], mesh.shape["tp"]
+
+    def run(*args):
+        rows, width = args[0].shape
+        hidden_here, depth = args[5].shape
+        fits = (
+            reps == 2
+            and cores == 2
+            and n % 2 == 0
+            and rows % ROWS == 0
+            and width % (2 * LANES) == 0
+            and depth % LANES == 0
+            and hidden_here % (2 * n * ROWS) == 0
+        )
+        return fast_shards(n, *args) if fits else shards(*args)
+
+    return run
+
+
 def solution(mesh):
     placed = (
         P(("rep", "fs"), None),
@@ -84,7 +483,7 @@
         P("tp", "fs"),
     )
     return jax.shard_map(
-        shards,
+        shards_for(mesh),
         mesh=mesh,
         in_specs=placed,
         out_specs=(

time: 609 us -> 290 us (0.48)
  waiting for transfers between devices: 521 us -> 0 us
  Pallas kernels: 0 us -> 220 us
  matrix products: 42.7 us -> 12.3 us
  other arithmetic: 10.9 us -> 35.9 us
  local copies, waits for them, and re-layouts: 4.6 us -> 18.9 us
  between operations: 14.3 us -> 1.01 us
  starting transfers between devices: 13.1 us -> 0 us
    all_gather x6 -> x0, waiting for transfers between devices: 420 us -> none  [the longest x1 97.5 us: shards(): lax.all_gather(w_up, 'fs', axis=0, tiled=True)]
    pallas_call x0 -> x5, Pallas kernels: none -> 220 us  [call(): pl.pallas_call(body, out_shape=outs, in_specs=[ANY] * len(args), out_spec...]
    psum x2 -> x0, waiting for transfers between devices: 87 us -> none  [the longest x1 68.2 us: shards(): lax.psum(gate_delta.astype(jnp.bfloat16), 'rep').astype(jnp.float32)]
    all_to_all x2 -> x0, starting transfers between devices: 12.6 us -> none  [the longest x1 6.53 us: shards(): lax.all_to_all(grad_out, 'fs', split_axis=1, concat_axis=0, tiled=True)]
    convert_element_type x3 -> x7, other arithmetic: 2.93 us -> 15.5 us  [the longest x3 12.6 us: fast_shards(): add = lambda a, b: (a.astype(f32) + b.astype(f32)).astype(bf16)]
    unnamed x20 -> x34, local copies, waits for them, and re-layouts: 0.04 us -> 12.6 us
    dot_general x3 -> x2, matrix products: 17 us -> 4.95 us  [the longest x1 2.85 us: fast_shards(): jnp.dot(hidden[tokens:], down_t, preferred_element_type=f32).astype(bf16)]
    all_to_all x2 -> x0, waiting for transfers between devices: 11.5 us -> none  [the longest x1 11.5 us: shards(): lax.all_to_all(early_normed, 'fs', split_axis=1, concat_axis=0, tiled=True)]
  transfers between devices with their start and end apart: 10 -> 0, of which waited for: 9 -> 0; matrix products, arithmetic and copies ran while one was open for 7% -> 0% of each run, Pallas kernels for 0% -> 0%
where the time goes in v1:
time: 290 us; the launch traced here: 288 us
  Pallas kernels  220 us (76%)
  other arithmetic  35.9 us (12%)
  local copies, waits for them, and re-layouts  18.9 us (7%)
  matrix products  12.3 us (4%)
    pallas_call x5, Pallas kernels, call(): pl.pallas_call(body, out_shape=outs, in_specs=[ANY] * len(args), out_spec...  220 us
    convert_element_type x3, other arithmetic, fast_shards(): add = lambda a, b: (a.astype(f32) + b.astype(f32)).astype(bf16)  12.6 us
    unnamed x34, local copies, waits for them, and re-layouts  12.6 us

profile of v1, /device:TPU:9, one launch (start us, length us, event | category | flops | bytes accessed | tf_op | source)
XLA Modules:
  0.0 288.3 jit_solution(18285372299147503441)
XLA Ops:
  7.6 1.6 pad_maximum_fusion.1.weights
  9.2 86.1 %shard_map.128 = (bf16[3,896,2048]{2,1,0:T(8,128)(2,1)}, bf16[3,192,2048]{2,1,0:T(8,128)(2,1)}) custom-call(bf16[3,112,2048]{2,1,0:T(8,128)(2,1)} %pad_maximum_fusion.3.acts, bf16[3,1536,256]{2,1,0:T(8,128)(2,1)} %pad_maximum_fusion.1.weights), custom_call_target="tpu_custom_call" | custom-call | tf_op jit(solution)/shard_map/pallas_call | solution.py:52
  95.3 4.6 %slice.53 = bf16[2,896,2048]{2,1,0:T(8,128)(2,1)S(1)} slice(bf16[3,896,2048]{2,1,0:T(8,128)(2,1)} %get-tuple-element.11), slice={[0:2], [0:896], [0:2048]} | slice | bytes 14680064 | tf_op jit(solution)/shard_map/slice | solution.py:331
  100.1 3.0 %fusion.53 = f32[1792,384]{0,1:T(8,128)S(1)} fusion(bf16[1792,2048]{1,0:T(8,128)(2,1)S(1)} %bitcast.87, bf16[384,2048]{1,0:T(8,128)(2,1)S(1)} %bitcast.93), kind=kOutput, calls=%fused_computation.81 | convolution fusion | flops 2818572288 | bytes 11665408 | tf_op jit(solution)/shard_map/dot_general | solution.py:23
  105.7 1.8 fusion.11
  108.6 1.7 pad_maximum_fusion.2
  110.2 2.1 convert_bitcast_fusion
  112.3 2.8 convert_bitcast_fusion.1
  115.2 1.9 copy-done.2
  117.1 3.6 %pad_maximum_fusion.parts = bf16[2,896,2048]{2,1,0:T(8,128)(2,1)} fusion(bf16[1,896,2048]{2,1,0:T(8,128)(2,1)S(1)} %convert_bitcast_fusion, bf16[1,896,2048]{2,1,0:T(8,128)(2,1)S(1)} %convert_bitcast_fusion.1), kind=kLoop, calls=%fused_computation.1 | loop fusion | flops 3670016 | bytes 14680064 | tf_op jit(solution)/shard_map/stack | solution.py:346
  120.7 29.0 %shard_map.129 = (bf16[2,896,1024]{2,1,0:T(8,128)(2,1)}, bf16[3,96,2048]{2,1,0:T(8,128)(2,1)}) custom-call(bf16[2,896,2048]{2,1,0:T(8,128)(2,1)} %pad_maximum_fusion.parts, bf16[3,192,2048]{2,1,0:T(8,128)(2,1)} %bitcast.85), custom_call_target="tpu_custom_call" | custom-call | tf_op jit(solution)/shard_map/pallas_call | solution.py:52
  149.7 2.7 add_convert_fusion.1.grads
  152.4 7.0 %add_convert_fusion = bf16[2,896,1024]{2,1,0:T(8,128)(2,1)} fusion(bf16[2,896,1024]{2,1,0:T(8,128)(2,1)} %get-tuple-element.13, s32[]{:T(128)S(6)} %select_n.32, bf16[1,896,2048]{2,1,0:T(8,128)(2,1)} %copy-done.2, bf16[1,896,2048]{2,1,0:T(8,128)(2,1)} %copy-done.1), kind=kLoop, calls=%fused_computation.3 | loop fusion | flops 12845056 | bytes 14680068 | tf_op jit(solution)/shard_map/convert_element_type | solution.py:355
  159.4 58.8 %shard_map.130 = (bf16[2,4,112,1024]{3,2,1,0:T(8,128)(2,1)}, bf16[3,1536,256]{2,1,0:T(8,128)(2,1)}) custom-call(bf16[2,4,2,112,1024]{4,3,2,1,0:T(8,128)(2,1)} %bitcast.83, bf16[3,96,2048]{2,1,0:T(8,128)(2,1)} %add_convert_fusion.1.grads), custom_call_target="tpu_custom_call" | custom-call | tf_op jit(solution)/shard_map/pallas_call | solution.py:52
  218.2 2.9 %fusion.1 = bf16[2,4,112,1024]{3,2,0,1:T(8,128)(2,1)S(1)} fusion(bf16[2,4,112,1024]{3,2,1,0:T(8,128)(2,1)} %get-tuple-element.15, bf16[2,4,2,112,1024]{4,3,2,1,0:T(8,128)(2,1)} %bitcast.84, s32[]{:T(128)S(6)} %select_n.33), kind=kLoop, calls=%fused_computation.6 | loop fusion | flops 3670016 | bytes 5505028 | tf_op jit(solution)/shard_map/convert_element_type | solution.py:355
  222.7 43.8 %shard_map.131 = bf16[3,2,112,1024]{3,2,1,0:T(8,128)(2,1)} custom-call(bf16[2,4,112,1024]{3,2,1,0:T(8,128)(2,1)} %copy.27.parts), custom_call_target="tpu_custom_call" | custom-call | tf_op jit(solution)/shard_map/pallas_call | solution.py:52
  266.5 1.7 convert_reduce_fusion
  269.1 2.5 shard_map.132
  275.3 1.6 copy.28
  276.9 3.0 %copy.29 = f32[256,1536]{0,1:T(8,128)} copy(f32[256,1536]{1,0:T(8,128)} %param.16) | data formatting | bytes 3145728 | tf_op args[7]
  279.9 2.7 fusion.20
  282.6 1.6 copy.30
  284.2 1.6 copy.31
  285.9 2.4 convert_add_fusion.1
  (47 shorter events, 16.6 us)
Async XLA Ops:
  0.6 4.0 %copy-start.5 = (bf16[112,2048]{1,0:T(8,128)(2,1)S(1)}, bf16[112,2048]{1,0:T(8,128)(2,1)}, u32[]{:S(2)}) copy-start(bf16[112,2048]{1,0:T(8,128)(2,1)} %param.11) | copy-start | bytes 1376260
  3.1 2.7 copy-start.10
  4.6 2.9 %copy-start.9 = (bf16[1536,256]{1,0:T(8,128)(2,1)S(1)}, bf16[1536,256]{1,0:T(8,128)(2,1)}, u32[]{:S(2)}) copy-start(bf16[1536,256]{1,0:T(8,128)(2,1)} %param.14) | copy-start | bytes 2359300
  95.3 4.6 %copy-start.8 = (bf16[3,192,2048]{2,1,0:T(8,128)(2,1)S(1)}, bf16[3,192,2048]{2,1,0:T(8,128)(2,1)}, u32[]{:S(2)}) copy-start(bf16[3,192,2048]{2,1,0:T(8,128)(2,1)} %get-tuple-element.12) | copy-start | bytes 7077892
  99.9 3.7 %slice-start = ((s8[11010048]{0:T(1024)(128)(4,1)}), s8[4194304]{0:T(1024)(128)(4,1)S(1)}, s32[]{:S(2)}) async-start(s8[11010048]{0:T(1024)(128)(4,1)} %bitcast.88), calls=%async_computation | async-start | bytes 8388608
  100.1 3.5 %slice-start.1 = ((s8[11010048]{0:T(1024)(128)(4,1)}), s8[4194304]{0:T(1024)(128)(4,1)S(1)}, s32[]{:S(2)}) async-start(s8[11010048]{0:T(1024)(128)(4,1)} %bitcast.88), calls=%async_computation.1 | async-start | bytes 8388608
  100.1 4.1 %slice-start.2 = ((s8[11010048]{0:T(1024)(128)(4,1)}), s8[2621440]{0:T(1024)(128)(4,1)S(1)}, s32[]{:S(2)}) async-start(s8[11010048]{0:T(1024)(128)(4,1)} %bitcast.88), calls=%async_computation.2 | async-start | bytes 5242880
  112.3 2.9 copy-start.1
  115.2 1.9 copy-start.2
  120.7 29.0 %copy-start = (bf16[576,2048]{1,0:T(8,128)(2,1)S(1)}, bf16[576,2048]{1,0:T(8,128)(2,1)}, u32[]{:S(2)}) copy-start(bf16[576,2048]{1,0:T(8,128)(2,1)} %pad_maximum_fusion.2) | copy-start | bytes 7077892
  271.6 1.5 copy-start.3
  272.9 1.0 copy-start.4
  273.4 1.9 copy-start.6
  284.2 1.6 copy-start.7

commit v2 on v1

--- a/solution.py
+++ b/solution.py
@@ -200,103 +200,193 @@
         push(ref, ref, send.at[side0 + place], recv.at[side0 + place], side).wait_send()
 
 
-def halves_kernel(parts, grads, parts_in, grads_in, send, recv):
-    rep, fs, tp, twin, mate = here()
-    half = parts.shape[2] // 2
-    part = grads.shape[1] // 2
-    greet([twin, mate])
-    one = push(
-        parts.at[:, :, block(1 - tp, half, LANES)], parts_in, send.at[0], recv.at[0], mate
-    )
-    two = push(grads.at[:, block(1 - rep, part, ROWS), :], grads_in, send.at[1], recv.at[1], twin)
-    one.start()
-    two.start()
-    one.wait()
-    two.wait()
-
-
-def pair_kernel(n, parts, grads, parts_in, grads_all, send, recv, stage, local):
-    rep, fs, tp, twin, mate = here()
-    y = lax.rem(fs, 2)
-    side = {"fs": fs + 1 - 2 * y}
-    part = grads.shape[1]
-    depth = grads_all.shape[2]
-    greet([twin] + [{"fs": lax.rem(fs + k, n)} for k in range(1, n)])
-    across = push(parts.at[:, :, 1 - y], parts_in, send.at[0], recv.at[0], side)
-
-    def slot(origin, who):
-        return grads_all.at[:, block(origin * 2 + who, part, ROWS), :]
-
-    def share(k):
-        to = lax.rem(fs + k, n)
-        src = grads.at[:, :, block(to, depth, LANES)]
-        return push(src, slot(fs, rep), send.at[k], recv.at[k], {"fs": to})
-
-    def share_on(k):
-        origin = lax.rem(fs + n - k, n)
-        return push(slot(origin, rep), slot(origin, rep), send.at[n + k], recv.at[n + k], twin)
-
-    def share_from_twin(k):
-        origin = lax.rem(fs + n - k, n)
-        ref = slot(origin, 1 - rep)
-        return push(ref, ref, send.at[n + k], recv.at[n + k], twin)
-
-    order = sorted(range(1, n), key=lambda k: -min(k, n - k))
-    for k in order:
-        share(k).start()
-    across.start()
-    own = grads.at[:, :, block(fs, depth, LANES)]
-    own_twin = push(own, slot(fs, rep), send.at[n], recv.at[n], twin)
-    own_twin.start()
-    take = pltpu.make_async_copy(own, stage, local.at[0])
-    take.start()
-    take.wait()
-    put = pltpu.make_async_copy(stage, slot(fs, rep), local.at[1])
-    put.start()
-    for k in order:
-        origin = lax.rem(fs + n - k, n)
-        ref = slot(origin, rep)
-        push(ref, ref, send.at[k], recv.at[k], twin).wait_recv()
-        share_on(k).start()
-    put.wait()
-    across.wait()
-    own_twin.wait_send()
-    ref = slot(fs, 1 - rep)
-    push(ref, ref, send.at[n], recv.at[n], twin).wait_recv()
-    for k in order:
-        share(k).wait_send()
-        share_on(k).wait_send()
-        share_from_twin(k).wait_recv()
-
-
-def line_kernel(n, parts, parts_in, send, recv):
+def add_rows(dst, left, right):
+    strip = ROWS
+    count = dst.shape[0] // strip
+
+    @pl.loop(0, count)
+    def _(i):
+        at = pl.ds(pl.multiple_of(i * strip, strip), strip)
+        total = left[at, :].astype(jnp.float32) + right[at, :].astype(jnp.float32)
+        dst[at, :] = total.astype(dst.dtype)
+
+
+def reduce_kernel(
+    n,
+    late,
+    norm,
+    gate_up,
+    down,
+    full,
+    grads_all,
+    p_in,
+    p2,
+    y_in,
+    p3,
+    z_in,
+    g_in,
+    g2,
+    sums,
+    send,
+    recv,
+    gsend,
+    grecv,
+    local,
+):
     rep, fs, tp, twin, mate = here()
     line = n // 2
-    z = fs // 2
-    greet([{"fs": lax.rem(fs + 2 * k, n)} for k in range(1, line)])
-
-    def copy(k):
-        to = lax.rem(z + k, line)
+    z, y = fs // 2, lax.rem(fs, 2)
+    side = {"fs": fs + 1 - 2 * y}
+    half = sums.shape[2]
+    rows = sums.shape[1]
+    part = g2.shape[1]
+    piece = 2 * part
+    depth = grads_all.shape[2]
+    mine, other = block(tp, half, LANES), block(1 - tp, half, LANES)
+    greet([twin, mate] + [{"fs": lax.rem(fs + k, n)} for k in range(1, n)])
+    order = sorted(range(1, line), key=lambda k: -min(k, line - k)) + [0]
+    far = sorted(range(1, n), key=lambda k: -min(k, n - k))
+    side0, line0, x0, last = 2 * line, 3 * line, 4 * line, 4 * line + 3
+
+    def place(k):
+        return lax.rem(z + k, line)
+
+    def span(k):
+        return block(place(k), 2 * rows, ROWS)
+
+    def to_mate(i, k):
+        src = (late, norm)[i].at[span(k), other]
+        at = i * line + k
+        return push(src, p_in.at[i, span(k), :], send.at[at], recv.at[at], mate)
+
+    def to_side(k):
+        src = p2.at[:, block(place(k) * 2 + 1 - y, rows, ROWS), :]
+        at = side0 + k
+        return push(src, y_in.at[:, place(k)], send.at[at], recv.at[at], side)
+
+    def to_line(k):
+        at = line0 + k
         return push(
-            parts.at[:, to],
-            parts_in.at[k - 1],
-            send.at[k],
-            recv.at[k],
-            {"fs": lax.rem(fs + 2 * k, n)},
+            p3.at[k], z_in.at[k - 1], send.at[at], recv.at[at], {"fs": lax.rem(fs + 2 * k, n)}
         )
 
-    for k in range(1, line):
-        copy(k).start()
-    for k in range(1, line):
-        copy(k).wait()
-
-
-def mate_kernel(sums, sums_in, send, recv):
-    rep, fs, tp, twin, mate = here()
-    greet([mate])
-    copy = push(sums, sums_in, send.at[0], recv.at[0], mate)
-    copy.start()
-    copy.wait()
+    def delta(a, who):
+        if a < 2:
+            return gate_up.at[block(2 * a + who, part, ROWS), :]
+        return down.at[block(who, part, ROWS), :]
+
+    def to_twin(a):
+        return push(delta(a, 1 - rep), g_in.at[a], send.at[x0 + a], recv.at[x0 + a], twin)
+
+    def slot(a, origin, who):
+        return grads_all.at[a, block(origin * 2 + who, part, ROWS), :]
+
+    def share(a, k):
+        to = lax.rem(fs + k, n)
+        src = g2.at[a, :, block(to, depth, LANES)]
+        at = a * n + k
+        return push(src, slot(a, fs, rep), gsend.at[at], grecv.at[at], {"fs": to})
+
+    def share_in(a, k):
+        ref = slot(a, lax.rem(fs + n - k, n), rep)
+        at = a * n + k
+        return push(ref, ref, gsend.at[at], grecv.at[at], twin)
+
+    def share_on(a, k):
+        ref = slot(a, lax.rem(fs + n - k, n), rep)
+        at = (3 + a) * n + k
+        return push(ref, ref, gsend.at[at], grecv.at[at], twin)
+
+    def share_from_twin(a, k):
+        ref = slot(a, lax.rem(fs + n - k, n), 1 - rep)
+        at = (3 + a) * n + k
+        return push(ref, ref, gsend.at[at], grecv.at[at], twin)
+
+    def own(a):
+        return g2.at[a, :, block(fs, depth, LANES)]
+
+    def own_twin(a):
+        at = (3 + a) * n
+        return push(own(a), slot(a, fs, rep), gsend.at[at], grecv.at[at], twin)
+
+    def own_put(a):
+        return pltpu.make_async_copy(own(a), slot(a, fs, rep), local.at[a])
+
+    def weight_step(a):
+        to_twin(a).wait_recv()
+        add_rows(g2.at[a], delta(a, rep), g_in.at[a])
+        for k in far:
+            share(a, k).start()
+        own_twin(a).start()
+        own_put(a).start()
+
+    def forward(a):
+        for k in far:
+            share_in(a, k).wait_recv()
+            share_on(a, k).start()
+
+    for k in order:
+        for i in range(2):
+            to_mate(i, k).start()
+    for a in range(3):
+        to_twin(a).start()
+    for k in order:
+        for i in range(2):
+            to_mate(i, k).wait_recv()
+            src = (late, norm)[i].at[span(k), mine]
+            add_rows(p2.at[i, span(k), :], src, p_in.at[i, span(k), :])
+        to_side(k).start()
+    weight_step(0)
+    for step, k in enumerate(order):
+        to_side(k).wait_recv()
+        for i in range(2):
+            src = p2.at[i, block(place(k) * 2 + y, rows, ROWS), :]
+            add_rows(p3.at[k, i], src, y_in.at[i, place(k)])
+        if k:
+            to_line(k).start()
+        if step < 2:
+            weight_step(step + 1)
+        if step >= 1:
+            if step - 1 < 3:
+                forward(step - 1)
+    for a in range(max(len(order) - 1, 0), 3):
+        forward(a)
+    for k in order[:-1]:
+        to_line(k).wait_recv()
+    for i in range(2):
+
+        @pl.loop(0, rows // ROWS)
+        def _(j):
+            at = pl.ds(pl.multiple_of(j * ROWS, ROWS), ROWS)
+            total = p3[0, i, at, :].astype(jnp.float32)
+            for k in range(1, line):
+                total += z_in[k - 1, i, at, :].astype(jnp.float32)
+            sums[i, at, :] = total.astype(sums.dtype)
+
+    out = push(sums, full.at[:, :, mine], send.at[last], recv.at[last], mate)
+    out.start()
+    keep = pltpu.make_async_copy(sums, full.at[:, :, mine], local.at[3])
+    keep.start()
+    for a in range(3):
+        own_put(a).wait()
+        own_twin(a).wait_send()
+        ref = slot(a, fs, 1 - rep)
+        at = (3 + a) * n
+        push(ref, ref, gsend.at[at], grecv.at[at], twin).wait_recv()
+        to_twin(a).wait_send()
+        for k in far:
+            share(a, k).wait_send()
+            share_on(a, k).wait_send()
+            share_from_twin(a, k).wait_recv()
+    for k in order:
+        for i in range(2):
+            to_mate(i, k).wait_send()
+        to_side(k).wait_send()
+        if k:
+            to_line(k).wait_send()
+    keep.wait()
+    out.wait_send()
+    push(sums, full.at[:, :, other], send.at[last], recv.at[last], mate).wait_recv()
 
 
 def fast_shards(n, x_early, x_late, grad_out, w_gate, w_up, w_down, gate_sum, up_sum, down_sum):
@@ -342,45 +432,34 @@
     normed_part = jnp.dot(grads_in, gate_up, preferred_element_type=f32).astype(bf16)
     gate_up_delta = contract_rows(grads_in, normed).astype(bf16)
     down_delta = (0.5 * contract_rows(hidden[:tokens], cotangent)).astype(bf16)
-    grads = jnp.concatenate([gate_up_delta, down_delta], axis=0).reshape(3, piece, width)
-    parts = jnp.stack([late_part, normed_part])
-    parts_in, grads_in = call(
-        halves_kernel,
-        [shape((2, tokens, half), bf16), shape((3, piece // 2, width), bf16)],
-        (2, 2),
-        1,
-        parts,
-        grads,
-    )
-    add = lambda a, b: (a.astype(f32) + b.astype(f32)).astype(bf16)
-    parts = add(lax.dynamic_slice_in_dim(parts, tp * half, half, 2), parts_in)
-    grads = add(lax.dynamic_slice_in_dim(grads, rep * (piece // 2), piece // 2, 1), grads_in)
-    parts = parts.reshape(2, line, 2, rows, half)
-    parts_in, grads_all = call(
-        functools.partial(pair_kernel, n),
-        [shape((2, line, rows, half), bf16), shape((3, hidden_here, depth), bf16)],
-        (2 * n, 2 * n),
-        2,
-        parts,
-        grads,
-        scratch=(
-            pltpu.VMEM((3, piece // 2, depth), bf16),
-            pltpu.SemaphoreType.DMA((2,)),
+    part = piece // 2
+    dma = pltpu.SemaphoreType.DMA
+    vmem = pl.BlockSpec(memory_space=pltpu.VMEM)
+    full, grads_all = pl.pallas_call(
+        functools.partial(reduce_kernel, n),
+        out_shape=[shape((2, rows, width), bf16), shape((3, hidden_here, depth), bf16)],
+        in_specs=[vmem] * 4,
+        out_specs=[ANY, ANY],
+        scratch_shapes=[
+            pltpu.VMEM((2, tokens, half), bf16),
+            pltpu.VMEM((2, tokens, half), bf16),
+            pltpu.VMEM((2, line, rows, half), bf16),
+            pltpu.VMEM((line, 2, rows, half), bf16),
+            pltpu.VMEM((line - 1, 2, rows, half), bf16),
+            pltpu.VMEM((3, part, width), bf16),
+            pltpu.VMEM((3, part, width), bf16),
+            pltpu.VMEM((2, rows, half), bf16),
+            dma((4 * line + 4,)),
+            dma((4 * line + 4,)),
+            dma((6 * n,)),
+            dma((6 * n,)),
+            dma((4,)),
+        ],
+        compiler_params=pltpu.CompilerParams(
+            collective_id=1, has_side_effects=True, vmem_limit_bytes=48 * 2**20
         ),
-    )
-    parts = add(lax.dynamic_index_in_dim(parts, y, 2, keepdims=False), parts_in)
-    parts_in = call(
-        functools.partial(line_kernel, n),
-        shape((line - 1, 2, rows, half), bf16),
-        (line, line),
-        3,
-        parts,
-    )
-    sums = lax.dynamic_index_in_dim(parts, fs // 2, 1, keepdims=False).astype(f32)
-    sums = (sums + jnp.sum(parts_in.astype(f32), axis=0)).astype(bf16)
-    sums_in = call(mate_kernel, shape((2, rows, half), bf16), (1, 1), 4, sums)
-    left, right = jnp.where(tp == 0, sums, sums_in), jnp.where(tp == 0, sums_in, sums)
-    full = jnp.concatenate([left, right], axis=2).astype(f32)
+    )(late_part, normed_part, gate_up_delta, down_delta)
+    full = full.astype(f32)
     branch, grad_normed = full[0], full[1]
     out_late = (late + 0.5 * branch).astype(bf16)
     unit_rows = early * early_scale
@@ -388,11 +467,12 @@
     grad_in = (
         grad_out.astype(f32) + early_scale * (grad_normed - unit_rows * inner)
     ).astype(bf16)
+    gate_delta, up_delta = lax.optimization_barrier((grads_all[0].T, grads_all[1].T))
     return (
         out_late,
         grad_in,
-        gate_sum + grads_all[0].T.astype(f32),
-        up_sum + grads_all[1].T.astype(f32),
+        gate_sum + gate_delta.astype(f32),
+        up_sum + up_delta.astype(f32),
         down_sum + grads_all[2].astype(f32),
     )
 

time: 290 us -> 233 us (0.80)
  Pallas kernels: 220 us -> 176 us
  other arithmetic: 35.9 us -> 16.2 us
    pallas_call x5 -> x1, Pallas kernels: 220 us -> 86.1 us  [call(): pl.pallas_call(body, out_shape=outs, in_specs=[ANY] * len(args), out_spec...]
    pallas_call x0 -> x1, Pallas kernels: none -> 90.2 us  [fast_shards(): pl.pallas_call(functools.partial(reduce_kernel, n), out_shape=[shape((2,...]
    convert_element_type x6 -> x1, other arithmetic: 14.1 us -> 0.2 us  [fast_shards(): full = full.astype(f32)]
    another operation x1 -> x0, other arithmetic: 3.58 us -> none  [fast_shards(): parts = jnp.stack([late_part, normed_part])]
    add x1 -> x2, other arithmetic: 2.69 us -> 5.8 us  [the longest x1 2.9 us: fast_shards(): up_sum + up_delta.astype(f32)]
    unnamed x34 -> x30, local copies, waits for them, and re-layouts: 12.6 us -> 14.8 us
where the time goes in v2:
time: 233 us; the launch traced here: 229 us
  Pallas kernels  176 us (76%)
  local copies, waits for them, and re-layouts  20.9 us (9%)
  other arithmetic  16.2 us (7%)
  matrix products  14.3 us (6%)
    pallas_call x1, Pallas kernels, fast_shards(): pl.pallas_call(functools.partial(reduce_kernel, n), out_shape=[shape((2,...  90.2 us
    pallas_call x1, Pallas kernels, call(): pl.pallas_call(body, out_shape=outs, in_specs=[ANY] * len(args), out_spec...  86.1 us
    unnamed x30, local copies, waits for them, and re-layouts  14.8 us

profile of v2, /device:TPU:9, one launch (start us, length us, event | category | flops | bytes accessed | tf_op | source)
XLA Modules:
  0.0 228.5 jit_solution(4236084451227975467)
XLA Ops:
  0.6 1.3 fusion.30
  1.9 1.2 fusion.31
  3.2 1.4 fusion.42
  4.6 1.2 pad_maximum_fusion.1.acts
  7.0 1.8 pad_maximum_fusion.weights
  8.8 86.1 %shard_map.128 = (bf16[3,896,2048]{2,1,0:T(8,128)(2,1)}, bf16[3,192,2048]{2,1,0:T(8,128)(2,1)}) custom-call(bf16[3,112,2048]{2,1,0:T(8,128)(2,1)} %pad_maximum_fusion.1.acts, bf16[3,1536,256]{2,1,0:T(8,128)(2,1)} %pad_maximum_fusion.weights), custom_call_target="tpu_custom_call" | custom-call | tf_op jit(solution)/shard_map/pallas_call | solution.py:52
  94.9 4.6 %slice.53 = bf16[2,896,2048]{2,1,0:T(8,128)(2,1)S(1)} slice(bf16[3,896,2048]{2,1,0:T(8,128)(2,1)} %get-tuple-element.11), slice={[0:2], [0:896], [0:2048]} | slice | bytes 14680064 | tf_op jit(solution)/shard_map/slice | solution.py:421
  99.7 3.0 %fusion.48 = f32[1792,384]{0,1:T(8,128)S(1)} fusion(bf16[1792,2048]{1,0:T(8,128)(2,1)S(1)} %bitcast.63, bf16[384,2048]{1,0:T(8,128)(2,1)S(1)} %bitcast.69), kind=kOutput, calls=%fused_computation.64 | convolution fusion | flops 2818572288 | bytes 11665408 | tf_op jit(solution)/shard_map/dot_general | solution.py:23
  103.7 1.5 fusion.41
  105.3 1.8 fusion.9.gate_up
  107.1 3.9 %convolution_convert_fusion.norm = bf16[896,2048]{1,0:T(8,128)(2,1)} fusion(bf16[384,2048]{1,0:T(8,128)(2,1)S(1)} %bitcast.70, bf16[896,192]{0,1:T(8,128)(2,1)S(1)} %get-tuple-element.23, bf16[896,192]{0,1:T(8,128)(2,1)S(1)} %get-tuple-element.22), kind=kOutput, calls=%fused_computation.7 | convolution fusion | flops 1412497408 | bytes 5931008 | tf_op jit(solution)/shard_map/dot_general | solution.py:432
  111.1 1.0 fusion.15.down
  112.1 3.0 %convolution_convert_fusion.1.late = bf16[896,2048]{1,0:T(8,128)(2,1)} fusion(bf16[3,192,2048]{2,1,0:T(8,128)(2,1)S(1)} %copy-done.2, bf16[1792,192]{0,1:T(8,128)(2,1)S(1)} %get-tuple-element.25), kind=kOutput, calls=%fused_computation.8 | convolution fusion | flops 706478080 | bytes 4800512 | tf_op jit(solution)/shard_map/dot_general | solution.py:426
  115.0 90.2 %shard_map.129 = (bf16[2,112,2048]{2,1,0:T(8,128)(2,1)S(1)}, bf16[3,1536,256]{2,1,0:T(8,128)(2,1)S(1)}) custom-call(bf16[896,2048]{1,0:T(8,128)(2,1)} %convolution_convert_fusion.1.late, bf16[896,2048]{1,0:T(8,128)(2,1)} %convolution_convert_fusion.norm, bf16[384,2048]{1,0:T(8,128)(2,1)S(1)} %fusion.9.gate_up, bf16[192,2048]{1,0:T(8,128)(2,1)S(1)} %fusion.15.down), custom_call_target="tpu_custom_call" | custom-call | tf_op jit(solution)/shard_map/pallas_call | solution.py:438
  205.3 1.2 slice_bitcast_fusion.1
  206.5 3.0 %copy.17 = f32[256,1536]{0,1:T(8,128)} copy(f32[256,1536]{1,0:T(8,128)} %param.16) | data formatting | bytes 3145728 | tf_op args[7]
  209.5 2.9 %convert_add_fusion.1 = f32[256,1536]{0,1:T(8,128)} fusion(f32[256,1536]{0,1:T(8,128)} %copy.17, bf16[256,1536]{0,1:T(8,128)(2,1)} %get-tuple-element.16), kind=kLoop, calls=%fused_computation.16 | loop fusion | flops 786432 | bytes 3932160 | tf_op jit(solution)/shard_map/add | solution.py:475
  212.4 3.0 %copy.19 = f32[256,1536]{1,0:T(8,128)} copy(f32[256,1536]{0,1:T(8,128)} %convert_add_fusion.1) | data formatting | bytes 3145728
  215.4 3.0 %copy.16 = f32[256,1536]{0,1:T(8,128)} copy(f32[256,1536]{1,0:T(8,128)} %param.15) | data formatting | bytes 3145728 | tf_op args[6]
  218.5 2.9 %convert_add_fusion.2 = f32[256,1536]{0,1:T(8,128)} fusion(f32[256,1536]{0,1:T(8,128)} %copy.16, bf16[256,1536]{0,1:T(8,128)(2,1)} %get-tuple-element.15), kind=kLoop, calls=%fused_computation.17 | loop fusion | flops 786432 | bytes 3932160 | tf_op jit(solution)/shard_map/add | solution.py:474
  221.4 3.0 %copy.18 = f32[256,1536]{1,0:T(8,128)} copy(f32[256,1536]{0,1:T(8,128)} %convert_add_fusion.2) | data formatting | bytes 3145728
  224.6 0.8 copy-done
  225.7 1.3 fusion.29
  227.2 1.3 convert_add_fusion
  (33 shorter events, 3.0 us)
Async XLA Ops:
  0.6 3.9 %copy-start.3 = (bf16[112,2048]{1,0:T(8,128)(2,1)S(1)}, bf16[112,2048]{1,0:T(8,128)(2,1)}, u32[]{:S(2)}) copy-start(bf16[112,2048]{1,0:T(8,128)(2,1)} %param.11) | copy-start | bytes 1376260
  4.5 1.3 copy-start.7
  4.6 1.9 copy-start.8
  5.8 1.2 copy-start.6
  94.8 4.6 %copy-start.2 = (bf16[3,192,2048]{2,1,0:T(8,128)(2,1)S(1)}, bf16[3,192,2048]{2,1,0:T(8,128)(2,1)}, u32[]{:S(2)}) copy-start(bf16[3,192,2048]{2,1,0:T(8,128)(2,1)} %get-tuple-element.12) | copy-start | bytes 7077892
  99.5 3.7 %slice-start = ((s8[11010048]{0:T(1024)(128)(4,1)}), s8[4194304]{0:T(1024)(128)(4,1)S(1)}, s32[]{:S(2)}) async-start(s8[11010048]{0:T(1024)(128)(4,1)} %bitcast.64), calls=%async_computation | async-start | bytes 8388608
  99.7 3.5 %slice-start.1 = ((s8[11010048]{0:T(1024)(128)(4,1)}), s8[4194304]{0:T(1024)(128)(4,1)S(1)}, s32[]{:S(2)}) async-start(s8[11010048]{0:T(1024)(128)(4,1)} %bitcast.64), calls=%async_computation.1 | async-start | bytes 8388608
  99.7 4.1 %slice-start.2 = ((s8[11010048]{0:T(1024)(128)(4,1)}), s8[2621440]{0:T(1024)(128)(4,1)S(1)}, s32[]{:S(2)}) async-start(s8[11010048]{0:T(1024)(128)(4,1)} %bitcast.64), calls=%async_computation.2 | async-start | bytes 5242880
  224.4 1.0 copy-start
  224.4 1.3 copy-start.1
  224.4 1.3 copy-start.4
  225.7 1.5 copy-start.5

commit v3 on v2

--- a/solution.py
+++ b/solution.py
@@ -55,7 +55,9 @@
         in_specs=[ANY] * len(args),
         out_specs=jax.tree.map(lambda _: ANY, outs),
         scratch_shapes=[pltpu.SemaphoreType.DMA((n,)) for n in sems] + list(scratch),
-        compiler_params=pltpu.CompilerParams(collective_id=collective, has_side_effects=True),
+        compiler_params=pltpu.CompilerParams(
+            collective_id=collective, has_side_effects=True, vmem_limit_bytes=2**20
+        ),
     )(*args)
 
 
@@ -389,6 +391,28 @@
     push(sums, full.at[:, :, other], send.at[last], recv.at[last], mate).wait_recv()
 
 
+def update_kernel(gate_sum, up_sum, down_sum, deltas, new_gate, new_up, new_down):
+    new_gate[...] = gate_sum[...] + deltas[0].astype(jnp.float32).T
+    new_up[...] = up_sum[...] + deltas[1].astype(jnp.float32).T
+    new_down[...] = down_sum[...] + deltas[2].astype(jnp.float32)
+
+
+def update(gate_sum, up_sum, down_sum, deltas):
+    depth, hidden_here = gate_sum.shape
+    step = next(b for b in (512, 256, 128) if hidden_here % b == 0)
+    wide = pl.BlockSpec((depth, step), lambda i: (0, i))
+    tall = pl.BlockSpec((step, depth), lambda i: (i, 0))
+    size = depth * hidden_here
+    return pl.pallas_call(
+        update_kernel,
+        grid=(hidden_here // step,),
+        out_shape=[jax.ShapeDtypeStruct(v.shape, v.dtype) for v in (gate_sum, up_sum, down_sum)],
+        in_specs=[wide, wide, tall, pl.BlockSpec((3, step, depth), lambda i: (0, i, 0))],
+        out_specs=[wide, wide, tall],
+        cost_estimate=pl.CostEstimate(flops=3 * size, bytes_accessed=30 * size, transcendentals=0),
+    )(gate_sum, up_sum, down_sum, deltas)
+
+
 def fast_shards(n, x_early, x_late, grad_out, w_gate, w_up, w_down, gate_sum, up_sum, down_sum):
     bf16, f32 = jnp.bfloat16, jnp.float32
     shape = jax.ShapeDtypeStruct
@@ -418,20 +442,23 @@
     gate_t, up_t, down_t = weights_all[0], weights_all[1], weights_all[2]
     normed, cotangent = acts_all[0], acts_all[2]
     gate_up = weights_all[:2].reshape(2 * piece, width)
-    pre = contract_cols(acts_all[:2].reshape(2 * n * rows, width), gate_up)
-    gate_pre, up_pre = pre[:, :piece], pre[:, piece:]
-    sig = jax.nn.sigmoid(gate_pre)
-    hidden = (gate_pre * sig * up_pre).astype(bf16)
+    def activations(rows_in):
+        pre = contract_cols(rows_in, gate_up)
+        gate_pre, up_pre = pre[:, :piece], pre[:, piece:]
+        sig = jax.nn.sigmoid(gate_pre)
+        return gate_pre, up_pre, sig, (gate_pre * sig * up_pre).astype(bf16)
+
     tokens = n * rows
-    late_part = jnp.dot(hidden[tokens:], down_t, preferred_element_type=f32).astype(bf16)
-    g, u, s = gate_pre[:tokens], up_pre[:tokens], sig[:tokens]
+    g, u, s, hidden = activations(normed)
+    hidden_late = activations(acts_all[1])[3]
+    late_part = jnp.dot(hidden_late, down_t, preferred_element_type=f32).astype(bf16)
     grad_hidden = 0.5 * contract_cols(cotangent, down_t)
     grad_gate_in = (grad_hidden * u * s * (1.0 + g * (1.0 - s))).astype(bf16)
     grad_up_in = (grad_hidden * g * s).astype(bf16)
     grads_in = jnp.concatenate([grad_gate_in, grad_up_in], axis=1)
     normed_part = jnp.dot(grads_in, gate_up, preferred_element_type=f32).astype(bf16)
     gate_up_delta = contract_rows(grads_in, normed).astype(bf16)
-    down_delta = (0.5 * contract_rows(hidden[:tokens], cotangent)).astype(bf16)
+    down_delta = (0.5 * contract_rows(hidden, cotangent)).astype(bf16)
     part = piece // 2
     dma = pltpu.SemaphoreType.DMA
     vmem = pl.BlockSpec(memory_space=pltpu.VMEM)
@@ -467,14 +494,7 @@
     grad_in = (
         grad_out.astype(f32) + early_scale * (grad_normed - unit_rows * inner)
     ).astype(bf16)
-    gate_delta, up_delta = lax.optimization_barrier((grads_all[0].T, grads_all[1].T))
-    return (
-        out_late,
-        grad_in,
-        gate_sum + gate_delta.astype(f32),
-        up_sum + up_delta.astype(f32),
-        down_sum + grads_all[2].astype(f32),
-    )
+    return (out_late, grad_in, *update(gate_sum, up_sum, down_sum, grads_all))
 
 
 def shards(x_early, x_late, grad_out, w_gate, w_up, w_down, gate_sum, up_sum, down_sum):
@@ -544,6 +564,7 @@
             and width % (2 * LANES) == 0
             and depth % LANES == 0
             and hidden_here % (2 * n * ROWS) == 0
+            and hidden_here % LANES == 0
         )
         return fast_shards(n, *args) if fits else shards(*args)
 

time: 233 us -> 211 us (0.906)
  local copies, waits for them, and re-layouts: 20.9 us -> 4.4 us
  other arithmetic: 16.2 us -> 5.04 us
  Pallas kernels: 176 us -> 181 us
    unnamed x30 -> x14, local copies, waits for them, and re-layouts: 14.8 us -> 4.3 us
    add x3 -> x0, other arithmetic: 7.15 us -> none  [the longest x1 2.9 us: fast_shards(): up_sum + up_delta.astype(f32)]
    pallas_call x0 -> x1, Pallas kernels: none -> 5.89 us  [update(): pl.pallas_call(update_kernel, grid=(hidden_here // step,), out_shape=[jax...]
    slice x1 -> x0, local copies, waits for them, and re-layouts: 4.62 us -> none  [fast_shards(): pre = contract_cols(acts_all[:2].reshape(2 * n * rows, width), gate_up)]
    dot_general x2 -> x3, matrix products: 4.56 us -> 5.14 us  [contract_cols(): lax.dot_general(left, right, (((1,), (1,)), ((), ())), preferred_element_...]
where the time goes in v3:
time: 211 us; the launch traced here: 207 us
  Pallas kernels  181 us (86%)
  matrix products  14.9 us (7%)
  other arithmetic  5.04 us (2%)
  local copies, waits for them, and re-layouts  4.4 us (2%)
    pallas_call x1, Pallas kernels, fast_shards(): pl.pallas_call(functools.partial(reduce_kernel, n), out_shape=[shape((2,...  90.5 us
    pallas_call x1, Pallas kernels, call(): pl.pallas_call(body, out_shape=outs, in_specs=[ANY] * len(args), out_spec...  85 us
    pallas_call x1, Pallas kernels, update(): pl.pallas_call(update_kernel, grid=(hidden_here // step,), out_shape=[jax...  5.89 us
    dot_general x3, matrix products, contract_cols(): lax.dot_general(left, right, (((1,), (1,)), ((), ())), preferred_element_...  5.14 us
    unnamed x14, local copies, waits for them, and re-layouts  4.3 us

profile of v3, /device:TPU:9, one launch (start us, length us, event | category | flops | bytes accessed | tf_op | source)
XLA Modules:
  0.0 206.6 jit_solution(4451161959627802324)
XLA Ops:
  0.6 1.3 fusion.36
  1.9 1.3 fusion.35
  3.2 1.4 copy.14
  4.7 0.3 copy.15
  5.0 0.3 pad_maximum_fusion.weights
  5.2 0.7 copy-done.1
  6.0 0.1 copy-done.2
  6.1 0.2 fusion.45
  6.3 0.8 copy-done.3
  7.1 0.2 pad_maximum_fusion.1.acts
  7.3 85.0 %shard_map.128 = (bf16[3,896,2048]{2,1,0:T(8,128)(2,1)S(1)}, bf16[3,192,2048]{2,1,0:T(8,128)(2,1)S(1)}) custom-call(bf16[3,112,2048]{2,1,0:T(8,128)(2,1)S(1)} %pad_maximum_fusion.1.acts, bf16[3,1536,256]{2,1,0:T(8,128)(2,1)S(1)} %pad_maximum_fusion.weights), custom_call_target="tpu_custom_call" | custom-call | tf_op jit(solution)/shard_map/pallas_call | solution.py:52
  92.4 1.8 fusion.2
  94.3 1.5 multiply_convert_fusion.2
  95.8 1.0 fusion.21.down
  96.8 1.8 fusion.8
  98.6 1.8 fusion.15.gate_up
  100.4 3.0 %convolution_convert_fusion.1.late = bf16[896,2048]{1,0:T(8,128)(2,1)} fusion(bf16[3,192,2048]{2,1,0:T(8,128)(2,1)S(1)} %get-tuple-element.13, f32[896,384]{0,1:T(8,128)S(1)} %fusion.8), kind=kOutput, calls=%fused_computation.12 | convolution fusion | flops 707510272 | bytes 5832704 | tf_op jit(solution)/shard_map/dot_general | solution.py:454
  103.4 3.9 %convolution_convert_fusion.norm = bf16[896,2048]{1,0:T(8,128)(2,1)} fusion(bf16[384,2048]{1,0:T(8,128)(2,1)S(1)} %bitcast.61, bf16[896,192]{0,1:T(8,128)(2,1)S(1)} %get-tuple-element.20, bf16[896,192]{0,1:T(8,128)(2,1)S(1)} %get-tuple-element.19), kind=kOutput, calls=%fused_computation.11 | convolution fusion | flops 1412497408 | bytes 5931008 | tf_op jit(solution)/shard_map/dot_general | solution.py:459
  107.4 90.5 %shard_map.129 = (bf16[2,112,2048]{2,1,0:T(8,128)(2,1)S(1)}, bf16[3,1536,256]{2,1,0:T(8,128)(2,1)S(1)}) custom-call(bf16[896,2048]{1,0:T(8,128)(2,1)} %convolution_convert_fusion.1.late, bf16[896,2048]{1,0:T(8,128)(2,1)} %convolution_convert_fusion.norm, bf16[384,2048]{1,0:T(8,128)(2,1)S(1)} %fusion.15.gate_up, bf16[192,2048]{1,0:T(8,128)(2,1)S(1)} %fusion.21.down), custom_call_target="tpu_custom_call" | custom-call | tf_op jit(solution)/shard_map/pallas_call | solution.py:465
  197.9 0.2 convert_element_type.60
  198.1 0.3 fusion.30
  198.4 0.9 copy-done
  199.3 1.4 fusion.34
  200.7 5.9 %shard_map.130 = (f32[256,1536]{1,0:T(8,128)}, f32[256,1536]{1,0:T(8,128)}, f32[1536,256]{1,0:T(8,128)}) custom-call(f32[256,1536]{1,0:T(8,128)} %gate_sum.1, f32[256,1536]{1,0:T(8,128)} %up_sum.1, f32[1536,256]{1,0:T(8,128)} %down_sum.1, bf16[3,1536,256]{2,1,0:T(8,128)(2,1)} %copy-done), custom_call_target="tpu_custom_call" | custom-call | flops 1179648 | bytes 11796480 | tf_op jit(solution)/shard_map/pallas_call | solution.py:406
  (12 shorter events, 0.1 us)
Async XLA Ops:
  0.6 4.0 %copy-start.5 = (bf16[256,1536]{1,0:T(8,128)(2,1)S(1)}, bf16[256,1536]{1,0:T(8,128)(2,1)}, u32[]{:S(2)}) copy-start(bf16[256,1536]{1,0:T(8,128)(2,1)} %param.13) | copy-start | bytes 2359300
  1.9 3.0 %copy-start.4 = (bf16[1536,256]{1,0:T(8,128)(2,1)S(1)}, bf16[1536,256]{1,0:T(8,128)(2,1)}, u32[]{:S(2)}) copy-start(bf16[1536,256]{1,0:T(8,128)(2,1)} %param.14) | copy-start | bytes 2359300
  5.0 1.0 copy-start.1
  5.0 1.1 copy-start.2
  6.1 1.0 copy-start.3
  197.9 1.4 copy-start

commit v4 on v3

--- a/solution.py
+++ b/solution.py
@@ -246,15 +246,13 @@
     depth = grads_all.shape[2]
     mine, other = block(tp, half, LANES), block(1 - tp, half, LANES)
     greet([twin, mate] + [{"fs": lax.rem(fs + k, n)} for k in range(1, n)])
-    order = sorted(range(1, line), key=lambda k: -min(k, line - k)) + [0]
+    order = sorted(range(line), key=lambda d: (-abs(2 * d + 1 - line), -d))
     far = sorted(range(1, n), key=lambda k: -min(k, n - k))
-    side0, line0, x0, last = 2 * line, 3 * line, 4 * line, 4 * line + 3
-
-    def place(k):
-        return lax.rem(z + k, line)
+    side0, line0, x0, last = 2 * line, 3 * line, 5 * line, 5 * line + 3
+    above, below = {"fs": lax.rem(fs + 2, n)}, {"fs": lax.rem(fs + n - 2, n)}
 
     def span(k):
-        return block(place(k), 2 * rows, ROWS)
+        return block(k, 2 * rows, ROWS)
 
     def to_mate(i, k):
         src = (late, norm)[i].at[span(k), other]
@@ -262,15 +260,44 @@
         return push(src, p_in.at[i, span(k), :], send.at[at], recv.at[at], mate)
 
     def to_side(k):
-        src = p2.at[:, block(place(k) * 2 + 1 - y, rows, ROWS), :]
+        src = p2.at[:, block(k * 2 + 1 - y, rows, ROWS), :]
         at = side0 + k
-        return push(src, y_in.at[:, place(k)], send.at[at], recv.at[at], side)
-
-    def to_line(k):
-        at = line0 + k
-        return push(
-            p3.at[k], z_in.at[k - 1], send.at[at], recv.at[at], {"fs": lax.rem(fs + 2 * k, n)}
-        )
+        return push(src, y_in.at[:, k], send.at[at], recv.at[at], side)
+
+    def go_up(d):
+        at = line0 + d
+        return push(p3.at[0, d], z_in.at[0, d], send.at[at], recv.at[at], above)
+
+    def go_down(d):
+        at = line0 + line + d
+        return push(p3.at[1, d], z_in.at[1, d], send.at[at], recv.at[at], below)
+
+    def chain(d):
+        to_side(d).wait_recv()
+
+        def make(way):
+            for i in range(2):
+                src = p2.at[i, block(d * 2 + y, rows, ROWS), :]
+                add_rows(p3.at[way, d, i], src, y_in.at[i, d])
+
+        def join(way, copy):
+            copy.wait_recv()
+            for i in range(2):
+                add_rows(p3.at[way, d, i], p3.at[way, d, i], z_in.at[way, d, i])
+
+        def rise():
+            make(0)
+            pl.when(z > 0)(lambda: join(0, go_up(d)))
+            go_up(d).start()
+
+        def fall():
+            make(1)
+            pl.when(z < line - 1)(lambda: join(1, go_down(d)))
+            go_down(d).start()
+
+        pl.when(z < d)(rise)
+        pl.when(z > d)(fall)
+        pl.when(z == d)(lambda: make(0))
 
     def delta(a, who):
         if a < 2:
@@ -340,12 +367,7 @@
         to_side(k).start()
     weight_step(0)
     for step, k in enumerate(order):
-        to_side(k).wait_recv()
-        for i in range(2):
-            src = p2.at[i, block(place(k) * 2 + y, rows, ROWS), :]
-            add_rows(p3.at[k, i], src, y_in.at[i, place(k)])
-        if k:
-            to_line(k).start()
+        chain(k)
         if step < 2:
             weight_step(step + 1)
         if step >= 1:
@@ -353,18 +375,25 @@
                 forward(step - 1)
     for a in range(max(len(order) - 1, 0), 3):
         forward(a)
-    for k in order[:-1]:
-        to_line(k).wait_recv()
-    for i in range(2):
-
-        @pl.loop(0, rows // ROWS)
-        def _(j):
-            at = pl.ds(pl.multiple_of(j * ROWS, ROWS), ROWS)
-            total = p3[0, i, at, :].astype(jnp.float32)
-            for k in range(1, line):
-                total += z_in[k - 1, i, at, :].astype(jnp.float32)
-            sums[i, at, :] = total.astype(sums.dtype)
-
+    for d in range(line):
+
+        def finish():
+            for way, there, copy in ((0, z > 0, go_up(d)), (1, z < line - 1, go_down(d))):
+
+                def join():
+                    copy.wait_recv()
+                    for i in range(2):
+                        add_rows(p3.at[0, d, i], p3.at[0, d, i], z_in.at[way, d, i])
+
+                pl.when(there)(join)
+            for i in range(2):
+
+                @pl.loop(0, rows // ROWS)
+                def _(j):
+                    at = pl.ds(pl.multiple_of(j * ROWS, ROWS), ROWS)
+                    sums[i, at, :] = p3[0, d, i, at, :]
+
+        pl.when(z == d)(finish)
     out = push(sums, full.at[:, :, mine], send.at[last], recv.at[last], mate)
     out.start()
     keep = pltpu.make_async_copy(sums, full.at[:, :, mine], local.at[3])
@@ -384,8 +413,8 @@
         for i in range(2):
             to_mate(i, k).wait_send()
         to_side(k).wait_send()
-        if k:
-            to_line(k).wait_send()
+        pl.when(z < k)(lambda: go_up(k).wait_send())
+        pl.when(z > k)(lambda: go_down(k).wait_send())
     keep.wait()
     out.wait_send()
     push(sums, full.at[:, :, other], send.at[last], recv.at[last], mate).wait_recv()
@@ -471,13 +500,13 @@
             pltpu.VMEM((2, tokens, half), bf16),
             pltpu.VMEM((2, tokens, half), bf16),
             pltpu.VMEM((2, line, rows, half), bf16),
-            pltpu.VMEM((line, 2, rows, half), bf16),
-            pltpu.VMEM((line - 1, 2, rows, half), bf16),
+            pltpu.VMEM((2, line, 2, rows, half), bf16),
+            pltpu.VMEM((2, line, 2, rows, half), bf16),
             pltpu.VMEM((3, part, width), bf16),
             pltpu.VMEM((3, part, width), bf16),
             pltpu.VMEM((2, rows, half), bf16),
-            dma((4 * line + 4,)),
-            dma((4 * line + 4,)),
+            dma((5 * line + 4,)),
+            dma((5 * line + 4,)),
             dma((6 * n,)),
             dma((6 * n,)),
             dma((4,)),

time: 211 us -> 220 us (1.043); the launches traced: 207 us -> 219 us
  Pallas kernels: 181 us -> 194 us
    pallas_call x1, Pallas kernels: 90.5 us -> 103 us  [fast_shards(): pl.pallas_call(functools.partial(reduce_kernel, n), out_shape=[shape((2,...]
where the time goes in v4:
time: 220 us; the launch traced here: 219 us
  Pallas kernels  194 us (88%)
  matrix products  14.9 us (7%)
  other arithmetic  5.04 us (2%)
  local copies, waits for them, and re-layouts  4.4 us (2%)
    pallas_call x1, Pallas kernels, fast_shards(): pl.pallas_call(functools.partial(reduce_kernel, n), out_shape=[shape((2,...  103 us
    pallas_call x1, Pallas kernels, call(): pl.pallas_call(body, out_shape=outs, in_specs=[ANY] * len(args), out_spec...  85 us
    pallas_call x1, Pallas kernels, update(): pl.pallas_call(update_kernel, grid=(hidden_here // step,), out_shape=[jax...  5.89 us
    dot_general x3, matrix products, contract_cols(): lax.dot_general(left, right, (((1,), (1,)), ((), ())), preferred_element_...  5.14 us

profile of v4, /device:TPU:9, one launch (start us, length us, event | category | flops | bytes accessed | tf_op | source)
XLA Modules:
  0.0 219.2 jit_solution(11936408020302970690)
XLA Ops:
  0.6 1.3 fusion.36
  1.9 1.3 fusion.35
  3.2 1.4 copy.14
  4.7 0.3 copy.15
  5.0 0.3 pad_maximum_fusion.weights
  5.2 0.7 copy-done.1
  6.0 0.1 copy-done.2
  6.1 0.2 fusion.45
  6.3 0.8 copy-done.3
  7.1 0.2 pad_maximum_fusion.1.acts
  7.3 85.0 %shard_map.128 = (bf16[3,896,2048]{2,1,0:T(8,128)(2,1)S(1)}, bf16[3,192,2048]{2,1,0:T(8,128)(2,1)S(1)}) custom-call(bf16[3,112,2048]{2,1,0:T(8,128)(2,1)S(1)} %pad_maximum_fusion.1.acts, bf16[3,1536,256]{2,1,0:T(8,128)(2,1)S(1)} %pad_maximum_fusion.weights), custom_call_target="tpu_custom_call" | custom-call | tf_op jit(solution)/shard_map/pallas_call | solution.py:52
  92.4 1.8 fusion.2
  94.3 1.5 multiply_convert_fusion.2
  95.8 1.0 fusion.21.down
  96.8 1.8 fusion.8
  98.6 1.8 fusion.15.gate_up
  100.4 3.0 %convolution_convert_fusion.1.late = bf16[896,2048]{1,0:T(8,128)(2,1)} fusion(bf16[3,192,2048]{2,1,0:T(8,128)(2,1)S(1)} %get-tuple-element.13, f32[896,384]{0,1:T(8,128)S(1)} %fusion.8), kind=kOutput, calls=%fused_computation.12 | convolution fusion | flops 707510272 | bytes 5832704 | tf_op jit(solution)/shard_map/dot_general | solution.py:483
  103.4 3.9 %convolution_convert_fusion.norm = bf16[896,2048]{1,0:T(8,128)(2,1)} fusion(bf16[384,2048]{1,0:T(8,128)(2,1)S(1)} %bitcast.61, bf16[896,192]{0,1:T(8,128)(2,1)S(1)} %get-tuple-element.20, bf16[896,192]{0,1:T(8,128)(2,1)S(1)} %get-tuple-element.19), kind=kOutput, calls=%fused_computation.11 | convolution fusion | flops 1412497408 | bytes 5931008 | tf_op jit(solution)/shard_map/dot_general | solution.py:488
  107.4 103.1 %shard_map.129 = (bf16[2,112,2048]{2,1,0:T(8,128)(2,1)S(1)}, bf16[3,1536,256]{2,1,0:T(8,128)(2,1)S(1)}) custom-call(bf16[896,2048]{1,0:T(8,128)(2,1)} %convolution_convert_fusion.1.late, bf16[896,2048]{1,0:T(8,128)(2,1)} %convolution_convert_fusion.norm, bf16[384,2048]{1,0:T(8,128)(2,1)S(1)} %fusion.15.gate_up, bf16[192,2048]{1,0:T(8,128)(2,1)S(1)} %fusion.21.down), custom_call_target="tpu_custom_call" | custom-call | tf_op jit(solution)/shard_map/pallas_call | solution.py:494
  210.5 0.2 convert_element_type.60
  210.7 0.3 fusion.30
  211.0 0.9 copy-done
  211.9 1.4 fusion.34
  213.3 5.9 %shard_map.130 = (f32[256,1536]{1,0:T(8,128)}, f32[256,1536]{1,0:T(8,128)}, f32[1536,256]{1,0:T(8,128)}) custom-call(f32[256,1536]{1,0:T(8,128)} %gate_sum.1, f32[256,1536]{1,0:T(8,128)} %up_sum.1, f32[1536,256]{1,0:T(8,128)} %down_sum.1, bf16[3,1536,256]{2,1,0:T(8,128)(2,1)} %copy-done), custom_call_target="tpu_custom_call" | custom-call | flops 1179648 | bytes 11796480 | tf_op jit(solution)/shard_map/pallas_call | solution.py:435
  (12 shorter events, 0.1 us)
Async XLA Ops:
  0.6 4.0 %copy-start.5 = (bf16[256,1536]{1,0:T(8,128)(2,1)S(1)}, bf16[256,1536]{1,0:T(8,128)(2,1)}, u32[]{:S(2)}) copy-start(bf16[256,1536]{1,0:T(8,128)(2,1)} %param.13) | copy-start | bytes 2359300
  1.9 3.0 %copy-start.4 = (bf16[1536,256]{1,0:T(8,128)(2,1)S(1)}, bf16[1536,256]{1,0:T(8,128)(2,1)}, u32[]{:S(2)}) copy-start(bf16[1536,256]{1,0:T(8,128)(2,1)} %param.14) | copy-start | bytes 2359300
  5.0 1.0 copy-start.1
  5.0 1.1 copy-start.2
  6.1 1.0 copy-start.3
  210.5 1.4 copy-start
